TPU v7x, 32 devices: a whole 2x2x4 slice. The times are simulated.
32 devices in a mesh: sp: 4 (over z), tp: 2 (over y), dp: 4 (over x, core).
Axes of the slice: x: 2, y: 2, z: 4, core: 2. Of those that a mesh axis runs over, the one named last changes fastest.
Arguments:
- latent: bfloat16 [5120, 3072], P(('dp', 'sp', 'tp')), parts along dimension 0, may hold values from -6 to 6
- condition: float32 [12288], P('dp'), parts along dimension 0, may hold values from -8 to 8
- ctx_condition: float32 [3072], replicated, may hold values from -8 to 8
- context: bfloat16 [512, 3072], P(('dp', 'sp')), parts along dimension 0, may hold values from -6 to 6
- mod_shift: bfloat16 [3072, 3072], P('sp', 'tp'), may hold values from -0.109375 to 0.109375
- mod_scale: bfloat16 [3072, 3072], P('sp', 'tp'), may hold values from -0.109375 to 0.109375
- mod_gate: bfloat16 [3072, 3072], P('sp', 'tp'), may hold values from -0.109375 to 0.109375
- norm_gain: float32 [3072], replicated, may hold values from 0.5 to 6
- w_query: bfloat16 [3072, 3072], P(None, 'tp'), may hold values from -0.109375 to 0.109375
- key_weight: bfloat16 [3072, 512], P(None, 'tp'), may hold values from -0.109375 to 0.109375
- value_weight: bfloat16 [3072, 512], P(None, 'tp'), may hold values from -0.109375 to 0.109375
- w_gate: bfloat16 [3072, 3072], P(None, 'tp'), may hold values from -0.109375 to 0.109375
- w_out: bfloat16 [3072, 3072], P('tp'), may hold values from -1.5 to 1.5
- sink_logit: float32 [48], P('tp'), may hold values from 4 to 7.5
Outputs:
- updated_latent: bfloat16 [5120, 3072], P(('dp', 'sp', 'tp')), parts along dimension 0
There are 4 independent parts, one for each index of `dp`. A program takes and returns all parts, laid end to end along the dimension named above; an argument that names none is the same for every part. Nothing has to cross between parts.
All inputs are finite; a program needn't handle non-finite values.
Results may differ from a plain program's by a relative error of at most 0.02.
The roundings to bfloat16 on the way count: a program that leaves them out, or rounds other values in their place, can miss the bound.
Values may be sent and summed in bfloat16 or wider, within the bound.
A program may use at most 128 MiB of HBM per device.

v0:
```python
import math
import jax
import jax.numpy as jnp
from jax import lax
from jax.sharding import PartitionSpec as P

HEAD_SIZE = 64
WINDOW = 128
GRID_W = 64
NORM_EPS = 1e-06
MASK_VALUE = -1e30


def with_halo(block, sides, width):
    for axis, dim in sides:
        count = lax.axis_size(axis)
        forward = [(i, i + 1) for i in range(count - 1)]
        backward = [(target, source) for source, target in forward]
        low = lax.ppermute(
            lax.slice_in_dim(block, block.shape[dim] - width, None, axis=dim), axis, forward
        )
        high = lax.ppermute(lax.slice_in_dim(block, 0, width, axis=dim), axis, backward)
        block = jnp.concatenate([low, block, high], axis=dim)
    return block


def modulate(row_data, gain_vec, shift_vec, scale_vec):
    values = row_data.astype(jnp.float32)
    inverse = lax.rsqrt(jnp.mean(values * values, axis=-1, keepdims=True) + NORM_EPS)
    return (values * inverse * gain_vec * (1.0 + scale_vec) + shift_vec).astype(jnp.bfloat16)


def rotate(projected, positions):
    row_count = projected.shape[0]
    head_count = projected.shape[1] // HEAD_SIZE
    quarter = HEAD_SIZE // 4
    half_dim = HEAD_SIZE // 2
    inverse = jnp.exp(-math.log(10000.0) * jnp.arange(quarter, dtype=jnp.float32) / quarter)
    grid_row = (positions // GRID_W).astype(jnp.float32)
    mesh_column = (positions % GRID_W).astype(jnp.float32)
    angles = jnp.concatenate([grid_row[:, None] * inverse, mesh_column[:, None] * inverse], axis=1)
    cosine = jnp.cos(angles)[:, None, :]
    sine_table = jnp.sin(angles)[:, None, :]
    shaped = projected.reshape(row_count, head_count, HEAD_SIZE)
    first_half = shaped[..., :half_dim]
    second = shaped[..., half_dim:]
    turned = jnp.concatenate(
        [first_half * cosine - second * sine_table, second * cosine + first_half * sine_table],
        axis=-1,
    )
    return turned.reshape(row_count, head_count * HEAD_SIZE)


def attend(
    queries, key_rows, value_rows, ctx_keys, ctx_values, sink_logit, q_begin, k_begin, seq_total
):
    row_count = queries.shape[0]
    key_count = key_rows.shape[0]
    ctx_count = ctx_keys.shape[0]
    kv_heads = key_rows.shape[1] // HEAD_SIZE
    head_count = queries.shape[1] // HEAD_SIZE
    group_size = head_count // kv_heads
    factor = 1.0 / math.sqrt(HEAD_SIZE)
    q_heads = queries.reshape(row_count, kv_heads, group_size, HEAD_SIZE)
    k_heads = key_rows.reshape(key_count, kv_heads, HEAD_SIZE)
    v_heads = value_rows.reshape(key_count, kv_heads, HEAD_SIZE)
    ck_heads = ctx_keys.reshape(ctx_count, kv_heads, HEAD_SIZE)
    cv_heads = ctx_values.reshape(ctx_count, kv_heads, HEAD_SIZE)
    near_scores = (
        jnp.einsum("qkgd,skd->kgqs", q_heads, k_heads, preferred_element_type=jnp.float32) * factor
    )
    q_pos = q_begin + jnp.arange(row_count, dtype=jnp.int32)
    k_pos = k_begin + jnp.arange(key_count, dtype=jnp.int32)
    in_window = (jnp.abs(q_pos[:, None] - k_pos[None, :]) <= WINDOW) & (
        (k_pos >= 0) & (k_pos < seq_total)
    )[None, :]
    near_scores = jnp.where(in_window, near_scores, MASK_VALUE)
    ctx_scores = (
        jnp.einsum("qkgd,skd->kgqs", q_heads, ck_heads, preferred_element_type=jnp.float32) * factor
    )
    sink_score = sink_logit.reshape(kv_heads, group_size)[:, :, None, None]
    peak_score = jnp.maximum(
        jnp.maximum(
            jnp.max(near_scores, axis=-1, keepdims=True),
            jnp.max(ctx_scores, axis=-1, keepdims=True),
        ),
        sink_score,
    )
    near_exp = jnp.exp(near_scores - peak_score)
    ctx_exp = jnp.exp(ctx_scores - peak_score)
    softmax_denominator = (
        jnp.sum(near_exp, axis=-1, keepdims=True)
        + jnp.sum(ctx_exp, axis=-1, keepdims=True)
        + jnp.exp(sink_score - peak_score)
    )
    near_weights = (near_exp / softmax_denominator).astype(jnp.bfloat16)
    ctx_weights = (ctx_exp / softmax_denominator).astype(jnp.bfloat16)
    result = jnp.einsum("kgqs,skd->qkgd", near_weights, v_heads, preferred_element_type=jnp.float32)
    result = result + jnp.einsum(
        "kgqs,skd->qkgd", ctx_weights, cv_heads, preferred_element_type=jnp.float32
    )
    return result.reshape(row_count, head_count * HEAD_SIZE)


def shards(
    latent,
    condition,
    ctx_condition,
    context,
    mod_shift,
    mod_scale,
    mod_gate,
    norm_gain,
    w_query,
    key_weight,
    value_weight,
    w_gate,
    w_out,
    sink_logit,
):
    sp_count = lax.axis_size("sp")
    sp_rank = lax.axis_index("sp")
    mod_rows = mod_shift.shape[0]
    cond_act = jax.nn.silu(condition).astype(jnp.bfloat16)
    ctx_act = jax.nn.silu(ctx_condition).astype(jnp.bfloat16)
    first_row = sp_rank * mod_rows
    lat_piece = lax.dynamic_slice_in_dim(cond_act, first_row, mod_rows, 0)
    ctx_piece = lax.dynamic_slice_in_dim(ctx_act, first_row, mod_rows, 0)
    both_conds = jnp.stack([lat_piece, ctx_piece])
    partial_value = jnp.concatenate(
        [
            jnp.dot(both_conds, mod_shift, preferred_element_type=jnp.float32),
            jnp.dot(both_conds, mod_scale, preferred_element_type=jnp.float32),
            jnp.dot(lat_piece[None, :], mod_gate, preferred_element_type=jnp.float32),
        ],
        axis=0,
    )
    summed = lax.psum(partial_value, "sp")
    vectors = lax.all_gather(summed, "tp", axis=1, tiled=True)
    lat_shift = vectors[0]
    ctx_shift = vectors[1]
    lat_scale = vectors[2]
    ctx_scale = vectors[3]
    lat_gate = vectors[4]
    hidden = modulate(latent, norm_gain, lat_shift, lat_scale)
    ctx_hidden = modulate(context, norm_gain, ctx_shift, ctx_scale)
    kv_width = key_weight.shape[1]
    q_width = w_query.shape[1]
    ctx_pair = jnp.concatenate(
        [
            jnp.dot(ctx_hidden, key_weight, preferred_element_type=jnp.float32).astype(
                jnp.bfloat16
            ),
            jnp.dot(ctx_hidden, value_weight, preferred_element_type=jnp.float32).astype(
                jnp.bfloat16
            ),
        ],
        axis=1,
    )
    ctx_all = lax.all_gather(ctx_pair, "sp", axis=0, tiled=True)
    row_piece = lax.all_gather(hidden, "tp", axis=0, tiled=True)
    projected = jnp.concatenate(
        [
            jnp.dot(row_piece, w_query, preferred_element_type=jnp.float32),
            jnp.dot(row_piece, key_weight, preferred_element_type=jnp.float32),
            jnp.dot(row_piece, value_weight, preferred_element_type=jnp.float32),
            jnp.dot(row_piece, w_gate, preferred_element_type=jnp.float32),
        ],
        axis=1,
    )
    block_rows = projected.shape[0]
    q_begin = sp_rank * block_rows
    positions = q_begin + jnp.arange(block_rows, dtype=jnp.int32)
    queries = rotate(projected[:, :q_width], positions).astype(jnp.bfloat16)
    key_rows = rotate(projected[:, q_width : q_width + kv_width], positions).astype(jnp.bfloat16)
    value_rows = projected[:, q_width + kv_width : q_width + 2 * kv_width].astype(jnp.bfloat16)
    gate_proj = projected[:, q_width + 2 * kv_width :].astype(jnp.bfloat16)
    key_value = jnp.concatenate([key_rows, value_rows], axis=1)
    padded = with_halo(key_value, (("sp", 0),), WINDOW)
    attended = attend(
        queries,
        padded[:, :kv_width],
        padded[:, kv_width:],
        ctx_all[:, :kv_width],
        ctx_all[:, kv_width:],
        sink_logit,
        q_begin,
        q_begin - WINDOW,
        block_rows * sp_count,
    )
    mixed = (attended * jax.nn.silu(gate_proj.astype(jnp.float32))).astype(jnp.bfloat16)
    branch = lax.psum_scatter(
        jnp.dot(mixed, w_out, preferred_element_type=jnp.float32).astype(jnp.bfloat16),
        "tp",
        scatter_dimension=0,
        tiled=True,
    ).astype(jnp.float32)
    return (latent.astype(jnp.float32) + lat_gate * branch).astype(jnp.bfloat16)


def solution(mesh):
    return jax.shard_map(
        shards,
        mesh=mesh,
        in_specs=(
            P(("dp", "sp", "tp"), None),
            P("dp"),
            P(),
            P(("dp", "sp"), None),
            P("sp", "tp"),
            P("sp", "tp"),
            P("sp", "tp"),
            P(),
            P(None, "tp"),
            P(None, "tp"),
            P(None, "tp"),
            P(None, "tp"),
            P("tp", None),
            P("tp"),
        ),
        out_specs=P(("dp", "sp", "tp"), None),
        check_vma=False,
    )
```

profile of v0, /device:TPU:0, one launch (start us, length us, event | category | flops | bytes accessed | tf_op | source)
XLA Modules:
  0.0 179.3 jit_solution(17299851433781400490)
XLA Ops:
  6.5 0.9 multiply_convert_fusion.1
  10.5 21.4 %psum.7 = f32[5,1536]{1,0:T(8,128)S(1)} all-reduce(f32[5,1536]{1,0:T(8,128)S(1)} %pad_maximum_fusion.5), channel_id=1, replica_groups=mesh['sp'=4,'tp'=2,'dp'=4] {'sp'}, use_global_device_ids=true, to_apply=%region_0.1 | all-reduce | flops 7680 | bytes 61440 | tf_op jit(solution)/shard_map/psum | solution.py:138
  31.9 4.8 %all_gather.9 = f32[5,3072]{1,0:T(8,128)S(1)} all-gather(f32[5,1536]{1,0:T(8,128)S(1)} %psum.7), channel_id=1, replica_groups=mesh['sp'=4,'tp'=2,'dp'=4] {'tp'}, dimensions={1}, use_global_device_ids=true | all-gather | bytes 92160 | tf_op jit(solution)/shard_map/all_gather | solution.py:139
  37.0 1.4 fusion.10
  39.1 1.8 %convolution_convert_fusion.3 = bf16[32,256]{1,0:T(8,128)(2,1)S(1)} fusion(bf16[3072,256]{1,0:T(8,128)(2,1)} %param.24, bf16[32,3072]{1,0:T(8,128)(2,1)S(1)} %copy-done.7, f32[3072]{0:T(1024)S(1)} %bitcast.93, f32[3072]{0:T(1024)S(1)} %bitcast.95, f32[3072]{0:T(1024)S(1)} %copy-done.9, f32[32]{0:T(128)S(1)} %add_rsqrt_fusion.1), kind=kOutput, calls=%fused_computation.30 | convolution fusion | flops 50929664 | bytes 1822848 | tf_op jit(solution)/shard_map/dot_general | solution.py:154
  41.0 13.4 %all_gather.11 = bf16[128,512]{1,0:T(8,128)(2,1)S(1)} all-gather(bf16[32,512]{1,0:T(8,128)(2,1)S(1)} %pad_maximum_fusion.7), channel_id=1, replica_groups=mesh['sp'=4,'tp'=2,'dp'=4] {'sp'}, dimensions={0}, use_global_device_ids=true | all-gather | bytes 163840 | tf_op jit(solution)/shard_map/all_gather | solution.py:160
  55.3 13.1 %all-gather.2.cloned.1.call-done = bf16[320,3072]{1,0:T(8,128)(2,1)} async-done(((bf16[160,3072]{1,0:T(8,128)(2,1)}), bf16[320,3072]{1,0:T(8,128)(2,1)}) %all-gather.2.cloned.1.call-update) | async-done | bytes 1966096 | tf_op jit(solution)/shard_map/all_gather | solution.py:161
  68.4 2.6 %fusion.38 = f32[320,256]{0,1:T(8,128)S(1)} fusion(bf16[320,3072]{1,0:T(8,128)(2,1)} %all-gather.2.cloned.1.call-done, bf16[3072,256]{1,0:T(8,128)(2,1)S(1)} %copy-done.8), kind=kOutput, calls=%fused_computation.87 | convolution fusion | flops 503316480 | bytes 3866624 | tf_op jit(solution)/shard_map/dot_general | solution.py:165
  71.3 2.8 %convolution_convert_fusion.2 = bf16[320,256]{1,0:T(8,128)(2,1)S(1)} fusion(bf16[320,3072]{1,0:T(8,128)(2,1)} %all-gather.2.cloned.1.call-done, bf16[3072,256]{1,0:T(8,128)(2,1)} %param.24), kind=kOutput, calls=%fused_computation.29 | convolution fusion | flops 503398400 | bytes 3702784 | tf_op jit(solution)/shard_map/dot_general | solution.py:166
  74.1 3.4 %collective-permute-start = (bf16[128,512]{1,0:T(8,128)(2,1)S(1)}, bf16[128,512]{1,0:T(8,128)(2,1)S(1)}, u32[]{:S(2)}, u32[]{:S(2)}) collective-permute-start(bf16[128,512]{1,0:T(8,128)(2,1)S(1)} %get-tuple-element.11), channel_id=1, source_target_pairs={{0,8},{8,16},{16,24},{1,9},{9,17},{17,25},{2,10},{10,18},{18,26},{... | collective-permute-start | bytes 393224 | tf_op jit(solution)/shard_map/ppermute | solution.py:19
  77.5 1.5 collective-permute-start.1
  79.0 7.7 %fusion.39 = f32[320,1536]{0,1:T(8,128)S(1)} fusion(bf16[320,3072]{1,0:T(8,128)(2,1)S(1)} %copy-done.11, bf16[3072,1536]{1,0:T(8,128)(2,1)} %param.22), kind=kOutput, calls=%fused_computation.88 | convolution fusion | flops 3019898880 | bytes 13369344 | tf_op jit(solution)/shard_map/dot_general | solution.py:164
  87.3 2.8 %bitcast_reduce_fusion = (f32[4,6,320]{2,1,0:T(8,128)S(1)}, f32[4,128,320,6]{1,2,3,0:T(8,128)}) fusion(bf16[128,4,64,1]{0,2,3,1:T(8,128)(2,1)S(1)} %bitcast.91, bf16[320,4,6,64]{0,3,2,1:T(8,128)(2,1)S(1)} %bitcast.83), kind=kOutput, calls=%fused_computation.8 | convolution fusion | flops 127787520 | bytes 5011456 | tf_op jit(solution)/shard_map/qkgd,skd->kgqs/dot_general | solution.py:79
  90.1 0.8 fusion.34
  90.9 1.2 copy.24
  92.1 4.5 %fusion.1 = (f32[4,6,320]{2,1,0:T(8,128)S(1)}, f32[4,576,320,6]{1,2,3,0:T(8,128)S(1)}) fusion(pred[320,576]{1,0:T(8,128)(4,1)S(1)} %fusion.14, bf16[576,4,64,1]{0,2,3,1:T(8,128)(2,1)S(1)} %bitcast.87, bf16[320,4,6,64]{0,3,2,1:T(8,128)(2,1)S(1)} %bitcast.84), kind=kOutput, calls=%fused_computation.4 | convolution fusion | flops 579494400 | bytes 19187712 | tf_op jit(solution)/shard_map/qkgd,skd->kgqs/dot_general | solution.py:70
  96.7 2.6 %fusion.4 = f32[4,6,320]{2,1,0:T(8,128)S(1)} fusion(f32[4,128,320,6]{1,2,3,0:T(8,128)S(1)} %copy-done.3, f32[4,6,320]{2,1,0:T(8,128)S(1)} %maximum_maximum_fusion), kind=kLoop, calls=%fused_computation.11 | loop fusion | flops 2941440 | bytes 3993600 | tf_op jit(solution)/shard_map/reduce_sum | solution.py:93
  99.3 5.5 %fusion = f32[4,6,320]{2,1,0:T(8,128)S(1)} fusion(f32[4,576,320,6]{1,2,3,0:T(8,128)S(1)} %get-tuple-element.25, f32[4,6,320]{2,1,0:T(8,128)S(1)} %maximum_maximum_fusion, pred[320,576]{1,0:T(8,128)(4,1)S(1)} %fusion.14), kind=kLoop, calls=%fused_computation.3 | loop fusion | flops 17687040 | bytes 17940480 | tf_op jit(solution)/shard_map/reduce_sum | solution.py:92
  105.0 5.7 %fusion.12 = f32[4,64,6,320]{3,1,2,0:T(8,128)S(1)} fusion(bf16[128,4,64,1]{0,2,3,1:T(8,128)(2,1)S(1)} %bitcast.96, f32[4,128,320,6]{1,2,3,0:T(8,128)} %get-tuple-element.27, f32[4,6,320]{2,1,0:T(8,128)S(1)} %exponential_add_fusion, f32[4,6,320]{2,1,0:T(8,128)S(1)} %maximum_maximum_fusion), kind=kOutput, calls=%fused_computation.24 | convolution fusion | flops 129761280 | bytes 6025216 | tf_op jit(solution)/shard_map/kgqs,skd->qkgd/dot_general | solution.py:99
  110.7 10.9 %fusion.13 = f32[4,64,6,320]{3,1,2,0:T(8,128)} fusion(f32[4,64,6,320]{3,1,2,0:T(8,128)S(1)} %fusion.12, bf16[576,4,64,1]{0,2,3,1:T(8,128)(2,1)S(1)} %bitcast.90, f32[4,576,320,6]{1,2,3,0:T(8,128)} %copy-done.2, f32[4,6,320]{2,1,0:T(8,128)S(1)} %exponential_add_fusion, f32[4,6,320]{2,1,0:T(8,128)S(1)} %maximum_maximum_fusion, pred[320,576]{1,0:T(8,128)(4,1)S(1)} %fusion.14), kind=kOutput, calls=%fused_computation.25 | convolution fusion | flops 588840960 | bytes 22167552 | tf_op jit(solution)/shard_map/kgqs,skd->qkgd/dot_general | solution.py:98
  121.6 2.0 %copy.28 = f32[320,1536]{1,0:T(8,128)S(1)} copy(f32[320,1536]{0,1:T(8,128)} %bitcast.85) | data formatting | bytes 3932160 | tf_op jit(solution)/shard_map/reshape | solution.py:102
  123.6 14.5 %convolution_convert_fusion = bf16[320,3072]{1,0:T(8,128)(2,1)} fusion(bf16[1536,3072]{1,0:T(8,128)(2,1)} %param.26, f32[320,1536]{1,0:T(8,128)S(1)} %copy.28, bf16[320,3072]{1,0:T(8,128)(2,1)} %all-gather.2.cloned.1.call-done, bf16[3072,1536]{1,0:T(8,128)(2,1)} %param.25), kind=kOutput, calls=%fused_computation.6 | convolution fusion | flops 6044712960 | bytes 24772608 | tf_op jit(solution)/shard_map/dot_general | solution.py:193
  138.2 31.8 %reduce-scatter.2.cloned.1.call-done = bf16[160,3072]{1,0:T(8,128)(2,1)} async-done(((bf16[320,3072]{1,0:T(8,128)(2,1)}), bf16[160,3072]{1,0:T(8,128)(2,1)}) %reduce-scatter.2.cloned.1.call-update) | async-done | bytes 983056 | tf_op jit(solution)/shard_map/reduce_scatter | solution.py:192
  170.0 2.5 %fusion.11 = bf16[160,3072]{1,0:T(8,128)(2,1)} fusion(bf16[160,3072]{1,0:T(8,128)(2,1)S(1)} %copy-done.4, bf16[160,3072]{1,0:T(8,128)(2,1)} %reduce-scatter.2.cloned.1.call-done, f32[3072]{0:T(1024)S(1)} %bitcast.97), kind=kLoop, calls=%fused_computation.22 | loop fusion | flops 2457600 | bytes 2961408 | tf_op jit(solution)/shard_map/convert_element_type | solution.py:198
  (66 shorter events, 6.1 us)
Async XLA Ops:
  6.5 1.7 copy-start
  6.5 61.9 %all-gather.2.cloned.1.call-start = ((), (), s32[]{:S(2)}) async-start(), calls=%async_computation.1 | async-start | bytes 2949120 | tf_op jit(solution)/shard_map/all_gather | solution.py:161
  6.5 2.4 %copy-start.5 = (bf16[768,1536]{1,0:T(8,128)(2,1)S(1)}, bf16[768,1536]{1,0:T(8,128)(2,1)}, u32[]{:S(2)}) copy-start(bf16[768,1536]{1,0:T(8,128)(2,1)} %param.18) | copy-start | bytes 7077892
  8.2 1.8 %copy-start.6 = (bf16[768,1536]{1,0:T(8,128)(2,1)S(1)}, bf16[768,1536]{1,0:T(8,128)(2,1)}, u32[]{:S(2)}) copy-start(bf16[768,1536]{1,0:T(8,128)(2,1)} %param.20) | copy-start | bytes 7077892
  8.9 27.8 %copy-start.4 = (bf16[160,3072]{1,0:T(8,128)(2,1)S(1)}, bf16[160,3072]{1,0:T(8,128)(2,1)}, u32[]{:S(2)}) copy-start(bf16[160,3072]{1,0:T(8,128)(2,1)} %param.14) | copy-start | bytes 2949124
  10.1 27.0 %copy-start.9 = (f32[3072]{0:T(1024)S(1)}, f32[3072]{0:T(1024)}, u32[]{:S(2)}) copy-start(f32[3072]{0:T(1024)} %param.21) | copy-start | bytes 36868
  10.5 28.0 %copy-start.7 = (bf16[32,3072]{1,0:T(8,128)(2,1)S(1)}, bf16[32,3072]{1,0:T(8,128)(2,1)}, u32[]{:S(2)}) copy-start(bf16[32,3072]{1,0:T(8,128)(2,1)} %param.17) | copy-start | bytes 589828
  10.5 28.2 %copy-start.8 = (bf16[3072,256]{1,0:T(8,128)(2,1)S(1)}, bf16[3072,256]{1,0:T(8,128)(2,1)}, u32[]{:S(2)}) copy-start(bf16[3072,256]{1,0:T(8,128)(2,1)} %param.23) | copy-start | bytes 4718596
  38.4 16.0 %copy-start.10 = (f32[24]{0:T(128)S(1)}, f32[24]{0:T(128)}, u32[]{:S(2)}) copy-start(f32[24]{0:T(128)} %param.27) | copy-start | bytes 292
  38.4 131.5 %reduce-scatter.2.cloned.1.call-start = ((), (), s32[]{:S(2)}) async-start(), calls=%async_computation.2 | async-start | bytes 2949120 | tf_op jit(solution)/shard_map/reduce_scatter | solution.py:192
  71.3 7.7 %copy-start.11 = (bf16[320,3072]{1,0:T(8,128)(2,1)S(1)}, bf16[320,3072]{1,0:T(8,128)(2,1)}, u32[]{:S(2)}) copy-start(bf16[320,3072]{1,0:T(8,128)(2,1)} %all-gather.2.cloned.1.call-done) | copy-start | bytes 5898244
  74.1 16.0 %collective-permute-start = (bf16[128,512]{1,0:T(8,128)(2,1)S(1)}, bf16[128,512]{1,0:T(8,128)(2,1)S(1)}, u32[]{:S(2)}, u32[]{:S(2)}) collective-permute-start(bf16[128,512]{1,0:T(8,128)(2,1)S(1)} %get-tuple-element.11), channel_id=1, source_target_pairs={{0,8},{8,16},{16,24},{1,9},{9,17},{17,25},{2,10},{10,18},{18,26},{... | collective-permute-start | bytes 393224 | tf_op jit(solution)/shard_map/ppermute | solution.py:19
  77.5 12.6 %collective-permute-start.1 = (bf16[128,512]{1,0:T(8,128)(2,1)S(1)}, bf16[128,512]{1,0:T(8,128)(2,1)S(1)}, u32[]{:S(2)}, u32[]{:S(2)}) collective-permute-start(bf16[128,512]{1,0:T(8,128)(2,1)S(1)} %get-tuple-element.12), channel_id=1, source_target_pairs={{8,0},{16,8},{24,16},{9,1},{17,9},{25,17},{10,2},{18,10},{26,18},{... | collective-permute-start | bytes 393224 | tf_op jit(solution)/shard_map/ppermute | solution.py:22
  92.1 4.6 %copy-start.3 = (f32[4,128,320,6]{1,2,3,0:T(8,128)S(1)}, f32[4,128,320,6]{1,2,3,0:T(8,128)}, u32[]{:S(2)}) copy-start(f32[4,128,320,6]{1,2,3,0:T(8,128)} %get-tuple-element.27) | copy-start | bytes 11796484
  96.6 8.1 %copy-start.2 = (f32[4,576,320,6]{1,2,3,0:T(8,128)}, f32[4,576,320,6]{1,2,3,0:T(8,128)S(1)}, u32[]{:S(2)}) copy-start(f32[4,576,320,6]{1,2,3,0:T(8,128)S(1)} %get-tuple-element.25) | copy-start | bytes 53084164
  138.2 34.3 %copy-start.1 = (bf16[768,1536]{1,0:T(8,128)(2,1)S(1)}, bf16[768,1536]{1,0:T(8,128)(2,1)}, u32[]{:S(2)}) copy-start(bf16[768,1536]{1,0:T(8,128)(2,1)} %param.19) | copy-start | bytes 7077892
Sparse Core Ops, SparseCore 0:
  38.6 29.8 all-gather.1
  138.3 31.6 reduce-scatter.1
where the time goes:
time: 180 us; the launch traced here: 179 us
  matrix products  55 us (31%)
  waiting for transfers between devices  44.9 us (25%)
  blocking collectives  39.5 us (22%)
  other arithmetic  14.8 us (8%)
  between operations  13.7 us (8%)
  local copies, waits for them, and re-layouts  6.34 us (4%)
  starting transfers between devices  4.91 us (3%)
    reduce_scatter x1, waiting for transfers between devices, shards(): lax.psum_scatter(jnp.dot(mixed, w_out, preferred_element_type=jnp.float32...  31.8 us
    psum x1, blocking collectives, shards(): summed = lax.psum(partial_value, 'sp')  21.4 us
    dot_general x1, matrix products, shards(): jnp.dot(mixed, w_out, preferred_element_type=jnp.float32)  14.5 us
    all_gather x1, blocking collectives, shards(): ctx_all = lax.all_gather(ctx_pair, 'sp', axis=0, tiled=True)  13.4 us
    all_gather x1, waiting for transfers between devices, shards(): row_piece = lax.all_gather(hidden, 'tp', axis=0, tiled=True)  13.1 us
    dot_general x1, matrix products, attend(): jnp.einsum('kgqs,skd->qkgd', near_weights, v_heads, preferred_element_typ...  10.9 us
    dot_general x1, matrix products, shards(): jnp.dot(row_piece, w_query, preferred_element_type=jnp.float32)  7.75 us
    dot_general x1, matrix products, attend(): jnp.einsum('kgqs,skd->qkgd', ctx_weights, cv_heads, preferred_element_typ...  5.69 us
  transfers between devices with their start and end apart: 4, of which 2 were waited for; matrix products, arithmetic and copies ran while one was open for 8% of the time, Pallas kernels for 0%

commit v1 on v0

--- a/solution.py
+++ b/solution.py
@@ -135,7 +135,9 @@
         ],
         axis=0,
     )
-    summed = lax.psum(partial_value, "sp")
+    summed = partial_value
+    for hop in (1, 2):
+        summed = summed + lax.ppermute(summed, "sp", [(dev, dev ^ hop) for dev in range(4)])
     vectors = lax.all_gather(summed, "tp", axis=1, tiled=True)
     lat_shift = vectors[0]
     ctx_shift = vectors[1]

time: 180 us -> 172 us (0.956)
  blocking collectives: 39.5 us -> 19.1 us
  waiting for transfers between devices: 44.9 us -> 52.2 us
  starting transfers between devices: 4.91 us -> 11.1 us
    psum x1 -> x0, blocking collectives: 21.4 us -> none  [shards(): summed = lax.psum(partial_value, 'sp')]
    ppermute x0 -> x2, starting transfers between devices: none -> 6.22 us  [shards(): lax.ppermute(summed, 'sp', [(dev, dev ^ hop) for dev in range(4)])]
    ppermute x0 -> x2, waiting for transfers between devices: none -> 3.81 us  [shards(): lax.ppermute(summed, 'sp', [(dev, dev ^ hop) for dev in range(4)])]
    all_gather x1, waiting for transfers between devices: 13.1 us -> 16.6 us  [shards(): row_piece = lax.all_gather(hidden, 'tp', axis=0, tiled=True)]
  transfers between devices with their start and end apart: 4 -> 6, of which waited for: 2 -> 4; matrix products, arithmetic and copies ran while one was open for 8% -> 8% of each run, Pallas kernels for 0% -> 0%
where the time goes in v1:
time: 172 us
  matrix products  53.7 us (31%)
  waiting for transfers between devices  52.2 us (30%)
  blocking collectives  19.1 us (11%)
  other arithmetic  14.8 us (9%)
  between operations  13.7 us (8%)
  starting transfers between devices  11.1 us (6%)
  local copies, waits for them, and re-layouts  7.18 us (4%)
    reduce_scatter x1, waiting for transfers between devices, shards(): lax.psum_scatter(jnp.dot(mixed, w_out, preferred_element_type=jnp.float32...  31.8 us
    all_gather x1, waiting for transfers between devices, shards(): row_piece = lax.all_gather(hidden, 'tp', axis=0, tiled=True)  16.6 us
    dot_general x1, matrix products, shards(): jnp.dot(mixed, w_out, preferred_element_type=jnp.float32)  14.5 us
    all_gather x1, blocking collectives, shards(): ctx_all = lax.all_gather(ctx_pair, 'sp', axis=0, tiled=True)  14.3 us
    dot_general x1, matrix products, attend(): jnp.einsum('kgqs,skd->qkgd', near_weights, v_heads, preferred_element_typ...  11 us
    dot_general x1, matrix products, shards(): jnp.dot(row_piece, w_query, preferred_element_type=jnp.float32)  7.75 us
    ppermute x2, starting transfers between devices, shards(): lax.ppermute(summed, 'sp', [(dev, dev ^ hop) for dev in range(4)])  6.22 us
    dot_general x1, matrix products, attend(): jnp.einsum('kgqs,skd->qkgd', ctx_weights, cv_heads, preferred_element_typ...  5.69 us
  transfers between devices with their start and end apart: 6, of which 4 were waited for; matrix products, arithmetic and copies ran while one was open for 8% of the time, Pallas kernels for 0%

profile of v1, /device:TPU:0, one launch (start us, length us, event | category | flops | bytes accessed | tf_op | source)
XLA Modules:
  0.0 171.9 jit_solution(6107371977890991749)
XLA Ops:
  10.5 3.1 %collective-permute-start = (f32[5,1536]{1,0:T(8,128)S(1)}, f32[5,1536]{1,0:T(8,128)S(1)}, u32[]{:S(2)}, u32[]{:S(2)}) collective-permute-start(f32[5,1536]{1,0:T(8,128)S(1)} %pad_maximum_fusion.5), channel_id=1, source_target_pairs={{0,8},{8,0},{16,24},{24,16},{1,9},{9,1},{17,25},{25,17},{2,10},{10... | collective-permute-start | bytes 92168 | tf_op jit(solution)/shard_map/ppermute | solution.py:140
  14.0 1.7 %collective-permute-done = f32[5,1536]{1,0:T(8,128)S(1)} collective-permute-done((f32[5,1536]{1,0:T(8,128)S(1)}, f32[5,1536]{1,0:T(8,128)S(1)}, u32[]{:S(2)}, u32[]{:S(2)}) %collective-permute-start) | collective-permute-done | bytes 30752 | tf_op jit(solution)/shard_map/ppermute | solution.py:140
  15.8 3.1 %collective-permute-start.1 = (f32[5,1536]{1,0:T(8,128)S(1)}, f32[5,1536]{1,0:T(8,128)S(1)}, u32[]{:S(2)}, u32[]{:S(2)}) collective-permute-start(f32[5,1536]{1,0:T(8,128)S(1)} %fusion.32), channel_id=1, source_target_pairs={{0,16},{8,24},{16,0},{24,8},{1,17},{9,25},{17,1},{25,9},{2,18},{10... | collective-permute-start | bytes 92168 | tf_op jit(solution)/shard_map/ppermute | solution.py:140
  18.9 2.1 %collective-permute-done.1 = f32[5,1536]{1,0:T(8,128)S(1)} collective-permute-done((f32[5,1536]{1,0:T(8,128)S(1)}, f32[5,1536]{1,0:T(8,128)S(1)}, u32[]{:S(2)}, u32[]{:S(2)}) %collective-permute-start.1) | collective-permute-done | bytes 30752 | tf_op jit(solution)/shard_map/ppermute | solution.py:140
  20.9 4.8 %all_gather.9 = f32[5,3072]{1,0:T(8,128)S(1)} all-gather(f32[5,1536]{1,0:T(8,128)S(1)} %add.157), channel_id=1, replica_groups=mesh['sp'=4,'tp'=2,'dp'=4] {'tp'}, dimensions={1}, use_global_device_ids=true | all-gather | bytes 92160 | tf_op jit(solution)/shard_map/all_gather | solution.py:141
  25.8 1.4 fusion.10
  29.1 14.3 %all_gather.11 = bf16[128,512]{1,0:T(8,128)(2,1)S(1)} all-gather(bf16[32,512]{1,0:T(8,128)(2,1)S(1)} %pad_maximum_fusion.7), channel_id=1, replica_groups=mesh['sp'=4,'tp'=2,'dp'=4] {'sp'}, dimensions={0}, use_global_device_ids=true | all-gather | bytes 163840 | tf_op jit(solution)/shard_map/all_gather | solution.py:162
  44.3 16.6 %all-gather.2.cloned.1.call-done = bf16[320,3072]{1,0:T(8,128)(2,1)} async-done(((bf16[160,3072]{1,0:T(8,128)(2,1)}), bf16[320,3072]{1,0:T(8,128)(2,1)}) %all-gather.2.cloned.1.call-update) | async-done | bytes 1966096 | tf_op jit(solution)/shard_map/all_gather | solution.py:163
  60.9 2.6 %fusion.39 = f32[320,256]{0,1:T(8,128)S(1)} fusion(bf16[320,3072]{1,0:T(8,128)(2,1)} %all-gather.2.cloned.1.call-done, bf16[3072,256]{1,0:T(8,128)(2,1)S(1)} %copy-done.8), kind=kOutput, calls=%fused_computation.88 | convolution fusion | flops 503316480 | bytes 3866624 | tf_op jit(solution)/shard_map/dot_general | solution.py:167
  63.8 2.8 %convolution_convert_fusion.2 = bf16[320,256]{1,0:T(8,128)(2,1)S(1)} fusion(bf16[320,3072]{1,0:T(8,128)(2,1)} %all-gather.2.cloned.1.call-done, bf16[3072,256]{1,0:T(8,128)(2,1)} %param.24), kind=kOutput, calls=%fused_computation.29 | convolution fusion | flops 503398400 | bytes 3702784 | tf_op jit(solution)/shard_map/dot_general | solution.py:168
  66.6 3.4 %collective-permute-start.2 = (bf16[128,512]{1,0:T(8,128)(2,1)S(1)}, bf16[128,512]{1,0:T(8,128)(2,1)S(1)}, u32[]{:S(2)}, u32[]{:S(2)}) collective-permute-start(bf16[128,512]{1,0:T(8,128)(2,1)S(1)} %get-tuple-element.11), channel_id=1, source_target_pairs={{0,8},{8,16},{16,24},{1,9},{9,17},{17,25},{2,10},{10,18},{18,26},{... | collective-permute-start | bytes 393224 | tf_op jit(solution)/shard_map/ppermute | solution.py:19
  70.0 1.5 collective-permute-start.3
  71.5 7.7 %fusion.40 = f32[320,1536]{0,1:T(8,128)S(1)} fusion(bf16[320,3072]{1,0:T(8,128)(2,1)S(1)} %copy-done.13, bf16[3072,1536]{1,0:T(8,128)(2,1)} %param.22), kind=kOutput, calls=%fused_computation.89 | convolution fusion | flops 3019898880 | bytes 13369344 | tf_op jit(solution)/shard_map/dot_general | solution.py:166
  79.8 2.8 %bitcast_reduce_fusion = (f32[4,6,320]{2,1,0:T(8,128)S(1)}, f32[4,128,320,6]{1,2,3,0:T(8,128)}) fusion(bf16[128,4,64,1]{0,2,3,1:T(8,128)(2,1)S(1)} %bitcast.91, bf16[320,4,6,64]{0,3,2,1:T(8,128)(2,1)S(1)} %bitcast.83), kind=kOutput, calls=%fused_computation.8 | convolution fusion | flops 127787520 | bytes 5011456 | tf_op jit(solution)/shard_map/qkgd,skd->kgqs/dot_general | solution.py:79
  83.4 1.2 copy.24
  84.6 4.5 %fusion.1 = (f32[4,6,320]{2,1,0:T(8,128)S(1)}, f32[4,576,320,6]{1,2,3,0:T(8,128)S(1)}) fusion(pred[320,576]{1,0:T(8,128)(4,1)S(1)} %fusion.14, bf16[576,4,64,1]{0,2,3,1:T(8,128)(2,1)S(1)} %bitcast.87, bf16[320,4,6,64]{0,3,2,1:T(8,128)(2,1)S(1)} %bitcast.84), kind=kOutput, calls=%fused_computation.4 | convolution fusion | flops 579494400 | bytes 19187712 | tf_op jit(solution)/shard_map/qkgd,skd->kgqs/dot_general | solution.py:70
  89.2 2.6 %fusion.4 = f32[4,6,320]{2,1,0:T(8,128)S(1)} fusion(f32[4,128,320,6]{1,2,3,0:T(8,128)S(1)} %copy-done.3, f32[4,6,320]{2,1,0:T(8,128)S(1)} %maximum_maximum_fusion), kind=kLoop, calls=%fused_computation.11 | loop fusion | flops 2941440 | bytes 3993600 | tf_op jit(solution)/shard_map/reduce_sum | solution.py:93
  91.8 5.5 %fusion = f32[4,6,320]{2,1,0:T(8,128)S(1)} fusion(f32[4,576,320,6]{1,2,3,0:T(8,128)S(1)} %get-tuple-element.25, f32[4,6,320]{2,1,0:T(8,128)S(1)} %maximum_maximum_fusion, pred[320,576]{1,0:T(8,128)(4,1)S(1)} %fusion.14), kind=kLoop, calls=%fused_computation.3 | loop fusion | flops 17687040 | bytes 17940480 | tf_op jit(solution)/shard_map/reduce_sum | solution.py:92
  97.6 5.7 %fusion.12 = f32[4,64,6,320]{3,1,2,0:T(8,128)S(1)} fusion(bf16[128,4,64,1]{0,2,3,1:T(8,128)(2,1)S(1)} %bitcast.96, f32[4,128,320,6]{1,2,3,0:T(8,128)} %get-tuple-element.27, f32[4,6,320]{2,1,0:T(8,128)S(1)} %exponential_add_fusion, f32[4,6,320]{2,1,0:T(8,128)S(1)} %maximum_maximum_fusion), kind=kOutput, calls=%fused_computation.24 | convolution fusion | flops 129761280 | bytes 6025216 | tf_op jit(solution)/shard_map/kgqs,skd->qkgd/dot_general | solution.py:99
  103.3 11.0 %fusion.13 = f32[4,64,6,320]{3,1,2,0:T(8,128)} fusion(f32[4,64,6,320]{3,1,2,0:T(8,128)S(1)} %fusion.12, bf16[576,4,64,1]{0,2,3,1:T(8,128)(2,1)S(1)} %bitcast.90, f32[4,576,320,6]{1,2,3,0:T(8,128)} %copy-done.2, f32[4,6,320]{2,1,0:T(8,128)S(1)} %exponential_add_fusion, f32[4,6,320]{2,1,0:T(8,128)S(1)} %maximum_maximum_fusion, pred[320,576]{1,0:T(8,128)(4,1)S(1)} %fusion.14), kind=kOutput, calls=%fused_computation.25 | convolution fusion | flops 588840960 | bytes 22167552 | tf_op jit(solution)/shard_map/kgqs,skd->qkgd/dot_general | solution.py:98
  114.2 2.0 %copy.28 = f32[320,1536]{1,0:T(8,128)S(1)} copy(f32[320,1536]{0,1:T(8,128)} %bitcast.85) | data formatting | bytes 3932160 | tf_op jit(solution)/shard_map/reshape | solution.py:102
  116.2 14.5 %convolution_convert_fusion = bf16[320,3072]{1,0:T(8,128)(2,1)} fusion(bf16[1536,3072]{1,0:T(8,128)(2,1)} %param.26, f32[320,1536]{1,0:T(8,128)S(1)} %copy.28, bf16[320,3072]{1,0:T(8,128)(2,1)} %all-gather.2.cloned.1.call-done, bf16[3072,1536]{1,0:T(8,128)(2,1)} %param.25), kind=kOutput, calls=%fused_computation.6 | convolution fusion | flops 6044712960 | bytes 24772608 | tf_op jit(solution)/shard_map/dot_general | solution.py:195
  130.8 31.8 %reduce-scatter.2.cloned.1.call-done = bf16[160,3072]{1,0:T(8,128)(2,1)} async-done(((bf16[320,3072]{1,0:T(8,128)(2,1)}), bf16[160,3072]{1,0:T(8,128)(2,1)}) %reduce-scatter.2.cloned.1.call-update) | async-done | bytes 983056 | tf_op jit(solution)/shard_map/reduce_scatter | solution.py:194
  162.6 2.5 %fusion.11 = bf16[160,3072]{1,0:T(8,128)(2,1)} fusion(bf16[160,3072]{1,0:T(8,128)(2,1)S(1)} %copy-done.4, bf16[160,3072]{1,0:T(8,128)(2,1)} %reduce-scatter.2.cloned.1.call-done, f32[3072]{0:T(1024)S(1)} %bitcast.97), kind=kLoop, calls=%fused_computation.22 | loop fusion | flops 2457600 | bytes 2961408 | tf_op jit(solution)/shard_map/convert_element_type | solution.py:200
  (75 shorter events, 9.1 us)
Async XLA Ops:
  6.5 1.7 copy-start
  6.5 54.4 %all-gather.2.cloned.1.call-start = ((), (), s32[]{:S(2)}) async-start(), calls=%async_computation.1 | async-start | bytes 2949120 | tf_op jit(solution)/shard_map/all_gather | solution.py:163
  6.5 2.4 %copy-start.5 = (bf16[768,1536]{1,0:T(8,128)(2,1)S(1)}, bf16[768,1536]{1,0:T(8,128)(2,1)}, u32[]{:S(2)}) copy-start(bf16[768,1536]{1,0:T(8,128)(2,1)} %param.18) | copy-start | bytes 7077892
  8.2 1.8 %copy-start.6 = (bf16[768,1536]{1,0:T(8,128)(2,1)S(1)}, bf16[768,1536]{1,0:T(8,128)(2,1)}, u32[]{:S(2)}) copy-start(bf16[768,1536]{1,0:T(8,128)(2,1)} %param.20) | copy-start | bytes 7077892
  8.9 4.7 %copy-start.4 = (bf16[160,3072]{1,0:T(8,128)(2,1)S(1)}, bf16[160,3072]{1,0:T(8,128)(2,1)}, u32[]{:S(2)}) copy-start(bf16[160,3072]{1,0:T(8,128)(2,1)} %param.14) | copy-start | bytes 2949124
  10.1 15.7 %copy-start.10 = (f32[3072]{0:T(1024)S(1)}, f32[3072]{0:T(1024)}, u32[]{:S(2)}) copy-start(f32[3072]{0:T(1024)} %param.21) | copy-start | bytes 36868
  10.5 16.7 %copy-start.12 = (f32[24]{0:T(128)S(1)}, f32[24]{0:T(128)}, u32[]{:S(2)}) copy-start(f32[24]{0:T(128)} %param.27) | copy-start | bytes 292
  10.5 17.1 %copy-start.7 = (bf16[32,3072]{1,0:T(8,128)(2,1)S(1)}, bf16[32,3072]{1,0:T(8,128)(2,1)}, u32[]{:S(2)}) copy-start(bf16[32,3072]{1,0:T(8,128)(2,1)} %param.17) | copy-start | bytes 589828
  10.5 17.5 %copy-start.8 = (bf16[3072,256]{1,0:T(8,128)(2,1)S(1)}, bf16[3072,256]{1,0:T(8,128)(2,1)}, u32[]{:S(2)}) copy-start(bf16[3072,256]{1,0:T(8,128)(2,1)} %param.23) | copy-start | bytes 4718596
  10.5 5.2 %collective-permute-start = (f32[5,1536]{1,0:T(8,128)S(1)}, f32[5,1536]{1,0:T(8,128)S(1)}, u32[]{:S(2)}, u32[]{:S(2)}) collective-permute-start(f32[5,1536]{1,0:T(8,128)S(1)} %pad_maximum_fusion.5), channel_id=1, source_target_pairs={{0,8},{8,0},{16,24},{24,16},{1,9},{9,1},{17,25},{25,17},{2,10},{10... | collective-permute-start | bytes 92168 | tf_op jit(solution)/shard_map/ppermute | solution.py:140
  15.8 5.2 %collective-permute-start.1 = (f32[5,1536]{1,0:T(8,128)S(1)}, f32[5,1536]{1,0:T(8,128)S(1)}, u32[]{:S(2)}, u32[]{:S(2)}) collective-permute-start(f32[5,1536]{1,0:T(8,128)S(1)} %fusion.32), channel_id=1, source_target_pairs={{0,16},{8,24},{16,0},{24,8},{1,17},{9,25},{17,1},{25,9},{2,18},{10... | collective-permute-start | bytes 92168 | tf_op jit(solution)/shard_map/ppermute | solution.py:140
  27.1 135.4 %reduce-scatter.2.cloned.1.call-start = ((), (), s32[]{:S(2)}) async-start(), calls=%async_computation.2 | async-start | bytes 2949120 | tf_op jit(solution)/shard_map/reduce_scatter | solution.py:194
  27.3 1.4 copy-start.9
  63.7 7.7 %copy-start.13 = (bf16[320,3072]{1,0:T(8,128)(2,1)S(1)}, bf16[320,3072]{1,0:T(8,128)(2,1)}, u32[]{:S(2)}) copy-start(bf16[320,3072]{1,0:T(8,128)(2,1)} %all-gather.2.cloned.1.call-done) | copy-start | bytes 5898244
  66.6 16.0 %collective-permute-start.2 = (bf16[128,512]{1,0:T(8,128)(2,1)S(1)}, bf16[128,512]{1,0:T(8,128)(2,1)S(1)}, u32[]{:S(2)}, u32[]{:S(2)}) collective-permute-start(bf16[128,512]{1,0:T(8,128)(2,1)S(1)} %get-tuple-element.11), channel_id=1, source_target_pairs={{0,8},{8,16},{16,24},{1,9},{9,17},{17,25},{2,10},{10,18},{18,26},{... | collective-permute-start | bytes 393224 | tf_op jit(solution)/shard_map/ppermute | solution.py:19
  70.0 12.6 %collective-permute-start.3 = (bf16[128,512]{1,0:T(8,128)(2,1)S(1)}, bf16[128,512]{1,0:T(8,128)(2,1)S(1)}, u32[]{:S(2)}, u32[]{:S(2)}) collective-permute-start(bf16[128,512]{1,0:T(8,128)(2,1)S(1)} %get-tuple-element.12), channel_id=1, source_target_pairs={{8,0},{16,8},{24,16},{9,1},{17,9},{25,17},{10,2},{18,10},{26,18},{... | collective-permute-start | bytes 393224 | tf_op jit(solution)/shard_map/ppermute | solution.py:22
  84.6 4.6 %copy-start.3 = (f32[4,128,320,6]{1,2,3,0:T(8,128)S(1)}, f32[4,128,320,6]{1,2,3,0:T(8,128)}, u32[]{:S(2)}) copy-start(f32[4,128,320,6]{1,2,3,0:T(8,128)} %get-tuple-element.27) | copy-start | bytes 11796484
  89.1 8.1 %copy-start.2 = (f32[4,576,320,6]{1,2,3,0:T(8,128)}, f32[4,576,320,6]{1,2,3,0:T(8,128)S(1)}, u32[]{:S(2)}) copy-start(f32[4,576,320,6]{1,2,3,0:T(8,128)S(1)} %get-tuple-element.25) | copy-start | bytes 53084164
  91.8 5.8 %copy-start.11 = (bf16[128,256]{0,1:T(8,128)(2,1)S(1)}, bf16[128,256]{0,1:T(8,128)(2,1)}, u32[]{:S(2)}) copy-start(bf16[128,256]{0,1:T(8,128)(2,1)} %copy.27) | copy-start | bytes 196612
  130.8 34.3 %copy-start.1 = (bf16[768,1536]{1,0:T(8,128)(2,1)S(1)}, bf16[768,1536]{1,0:T(8,128)(2,1)}, u32[]{:S(2)}) copy-start(bf16[768,1536]{1,0:T(8,128)(2,1)} %param.19) | copy-start | bytes 7077892
Sparse Core Ops, SparseCore 0:
  27.3 33.5 all-gather.1
  130.9 31.6 reduce-scatter.1
